TPU v7x, 32 devices: a whole 2x2x4 slice. The times are simulated.
32 devices in a mesh: grp: 2 (over y), sp: 4 (over z), tp: 4 (over x, core).
Axes of the slice: x: 2, y: 2, z: 4, core: 2. Of those that a mesh axis runs over, the one named last changes fastest.
Arguments:
- stream: bfloat16 [6144, 4096], P(('grp', 'sp'), 'tp'), parts along dimension 0, may hold values from -400 to 400
- in_weight: bfloat16 [2, 1024, 4096], P(None, 'sp', 'tp'), may hold values from -0.09375 to 0.09375
- out_weight: bfloat16 [2, 1024, 4096], P(None, 'sp', 'tp'), may hold values from -0.1875 to 0.1875
- group_mix: bfloat16 [2, 4, 256, 256], replicated, may hold values from -0.375 to 0.375
- pool_gain: float32 [2, 1024], replicated, may hold values from 0.1 to 1.9
- norm_gain: float32 [2, 4096], P(None, 'tp'), may hold values from 0.1 to 1.9
- norm_shift: float32 [2, 4096], P(None, 'tp'), may hold values from -3 to 3
Outputs:
- refined: bfloat16 [6144, 4096], P(('grp', 'sp'), 'tp'), parts along dimension 0
There are 2 independent parts, one for each index of `grp`. A program takes and returns all parts, laid end to end along the dimension named above; an argument that names none is the same for every part. Nothing has to cross between parts.
All inputs are finite; a program needn't handle non-finite values.
Results may differ from a plain program's by a relative error of at most 0.015.
Values may be sent and summed in bfloat16 or wider, within the bound.
A program may use at most 64 MiB of HBM per device.

v0:
```python
import jax
import jax.numpy as jnp
from jax import lax
from jax.sharding import PartitionSpec as P

D = 4096
POOL = 1024
GROUPS = 4
GROUP_WIDTH = 256
LAYERS = 2
epsilon = 1e-05


def passed_along(block, axis, distance):
    devices = range(lax.axis_size(axis))
    route = [(i - distance, i) for i in devices if i - distance in devices]
    return lax.ppermute(block, axis, route)


def pooled_windows(hidden, tok_start):
    reach = 2**GROUPS - 1
    length = hidden.shape[1]
    channels = hidden.shape[0]
    earlier = passed_along(hidden[:, length - reach :], "sp", 1)
    extended = jnp.concatenate([earlier, hidden], axis=1).astype(jnp.float32)
    group_ids = (jnp.arange(channels, dtype=jnp.int32) // GROUP_WIDTH)[:, None]
    running = extended
    window_sums = jnp.zeros((channels, length), jnp.float32)
    for octave in range(GROUPS):
        offset = 2**octave
        running = running[:, offset:] + running[:, : running.shape[1] - offset]
        window_sums = jnp.where(
            group_ids == octave, running[:, running.shape[1] - length :], window_sums
        )
    positions = (tok_start + jnp.arange(length, dtype=jnp.int32) + 1).astype(jnp.float32)
    widths = jnp.exp2((group_ids + 1).astype(jnp.float32))
    counts = jnp.minimum(positions[None, :], widths)
    return (window_sums / counts - hidden.astype(jnp.float32)).astype(jnp.bfloat16)


def per_device(stream, in_weight, out_weight, group_mix, pool_gain, norm_gain, norm_shift):
    tok_rows = stream.shape[0]
    tok_start = lax.axis_index("sp") * tok_rows
    alpha = (2.0 * LAYERS) ** 0.25
    contract_rows = (((0,), (0,)), ((), ()))
    contract_cols = (((1,), (1,)), ((), ()))
    current = stream
    for layer_index in range(LAYERS):
        whole_in = lax.all_gather(in_weight[layer_index], "sp", axis=0, tiled=True)
        partial_value = lax.dot_general(
            whole_in, current, contract_cols, preferred_element_type=jnp.float32
        )
        hidden = lax.psum(partial_value.astype(jnp.bfloat16), "tp")
        pooled = pooled_windows(hidden, tok_start)
        grouped = pooled.reshape(GROUPS, GROUP_WIDTH, tok_rows)
        mixed = jnp.einsum(
            "gio,git->got", group_mix[layer_index], grouped, preferred_element_type=jnp.float32
        )
        gains = pool_gain[layer_index].reshape(GROUPS, GROUP_WIDTH, 1)
        scaled = (mixed * gains).astype(jnp.bfloat16).reshape(POOL, tok_rows)
        branch = lax.dot_general(
            scaled,
            lax.all_gather(out_weight[layer_index], "sp", axis=0, tiled=True),
            contract_rows,
            preferred_element_type=jnp.float32,
        )
        summed = alpha * current.astype(jnp.float32) + branch
        row_sum, row_squares = lax.psum(
            (jnp.sum(summed, axis=1), jnp.sum(summed * summed, axis=1)), "tp"
        )
        row_mean = row_sum / D
        row_var = row_squares / D - row_mean * row_mean
        normed = (summed - row_mean[:, None]) * lax.rsqrt(row_var + epsilon)[:, None]
        current = (
            normed * norm_gain[layer_index][None, :] + norm_shift[layer_index][None, :]
        ).astype(jnp.bfloat16)
    return current


def solution(mesh):
    in_specs = (
        P(("grp", "sp"), "tp"),
        P(None, "sp", "tp"),
        P(None, "sp", "tp"),
        P(),
        P(),
        P(None, "tp"),
        P(None, "tp"),
    )
    out_specs = P(("grp", "sp"), "tp")
    return jax.shard_map(
        per_device, mesh=mesh, in_specs=in_specs, out_specs=out_specs, check_vma=False
    )
```

profile of v0, /device:TPU:0, one launch (start us, length us, event | category | flops | bytes accessed | tf_op | source)
XLA Modules:
  0.0 312.8 jit_solution(13905823871252964514)
XLA Ops:
  6.5 0.0 all-gather.9.cloned.1.call-start
  6.5 2.2 fusion.49
  8.8 0.0 all-gather.9.cloned.1.call-update
  8.8 0.0 copy-start.2
  8.8 0.0 all-reduce.5.cloned.1.call-start
  8.9 48.5 %all-gather.9.cloned.1.call-done = bf16[1,1024,1024]{2,1,0:T(8,128)(2,1)} async-done(((bf16[1,256,1024]{2,1,0:T(8,128)(2,1)}), bf16[1,1024,1024]{2,1,0:T(8,128)(2,1)}) %all-gather.9.cloned.1.call-update) | async-done | bytes 2097168 | tf_op jit(solution)/shard_map/all_gather | solution.py:49
  57.3 5.0 %fusion.22 = bf16[1024,768]{1,0:T(8,128)(2,1)} fusion(bf16[768,1024]{1,0:T(8,128)(2,1)} %param.7, bf16[1,1024,1024]{2,1,0:T(8,128)(2,1)} %all-gather.9.cloned.1.call-done), kind=kOutput, calls=%fused_computation.40 | convolution fusion | flops 1611399168 | bytes 5242880 | tf_op jit(solution)/shard_map/dot_general | solution.py:50
  62.3 0.0 copy-start.4
  62.3 0.0 copy-start.5
  62.3 0.0 copy-start.6
  62.4 0.0 all-reduce.5.cloned.1.call-update
  62.4 0.0 all-gather.11.cloned.1.call-start
  62.4 0.0 copy-done.2
  62.4 1.1 fusion.48
  63.5 0.0 all-gather.11.cloned.1.call-update
  63.5 0.0 all-gather.13.cloned.1.call-start
  63.6 0.5 all-gather.13.cloned.1.call-update
  64.1 0.0 all-reduce.7.cloned.1.call-start
  64.2 0.0 copy-done.4
  64.3 0.0 copy-done.5
  64.3 0.0 copy-done.6
  64.3 39.9 %all-reduce.5.cloned.1.call-done = bf16[1024,768]{1,0:T(8,128)(2,1)} async-done(((bf16[1024,768]{1,0:T(8,128)(2,1)}), bf16[1024,768]{1,0:T(8,128)(2,1)}) %all-reduce.5.cloned.1.call-update) | async-done | bytes 1572880 | tf_op jit(solution)/shard_map/psum | solution.py:53
  104.2 1.1 slice.138
  105.3 3.4 %collective-permute-start = (bf16[1024,15]{1,0:T(8,128)(2,1)S(1)}, bf16[1024,15]{1,0:T(8,128)(2,1)S(1)}, u32[]{:S(2)}, u32[]{:S(2)}) collective-permute-start(bf16[1024,15]{1,0:T(8,128)(2,1)S(1)} %slice.138), channel_id=1, source_target_pairs={{0,4},{4,8},{8,12},{1,5},{5,9},{9,13},{2,6},{6,10},{10,14},{3,7},{... | collective-permute-start | bytes 92168 | tf_op jit(solution)/shard_map/ppermute | solution.py:17
  108.7 5.4 %collective-permute-done = bf16[1024,15]{1,0:T(8,128)(2,1)S(1)} collective-permute-done((bf16[1024,15]{1,0:T(8,128)(2,1)S(1)}, bf16[1024,15]{1,0:T(8,128)(2,1)S(1)}, u32[]{:S(2)}, u32[]{:S(2)}) %collective-permute-start) | collective-permute-done | bytes 30752 | tf_op jit(solution)/shard_map/ppermute | solution.py:17
  114.1 2.3 maximum_convert_fusion
  116.4 1.0 slice_add_fusion.5
  117.4 1.0 slice_add_fusion.4
  118.5 0.0 copy-start
  118.5 1.0 slice_add_fusion.3
  119.5 0.4 copy-done
  119.9 0.0 copy-start.3
  119.9 4.1 %fusion.1 = bf16[1024,768]{1,0:T(8,128)(2,1)S(1)} fusion(f32[1024,782]{1,0:T(8,128)S(1)} %slice_add_fusion.5, f32[1024,780]{1,0:T(8,128)S(1)} %slice_add_fusion.4, f32[1024,776]{1,0:T(8,128)S(1)} %slice_add_fusion.3, bf16[1024,768]{1,0:T(8,128)(2,1)S(1)} %copy-done, f32[1024]{0:T(1024)S(1)} %fusion.44, f32[768]{0:T(1024)S(1)} %add_convert_fusion.2, ...), kind=kLoop, calls=%fused_computation.9 | loop fusion | flops 7864320 | bytes 15739904 | tf_op jit(solution)/shard_map/convert_element_type | solution.py:38
  124.0 0.0 copy-done.3
  124.0 0.6 multiply_convert_fusion.1
  124.7 26.8 %all-gather.11.cloned.1.call-done = bf16[1,1024,1024]{2,1,0:T(8,128)(2,1)} async-done(((bf16[1,256,1024]{2,1,0:T(8,128)(2,1)}), bf16[1,1024,1024]{2,1,0:T(8,128)(2,1)}) %all-gather.11.cloned.1.call-update) | async-done | bytes 2097168 | tf_op jit(solution)/shard_map/all_gather | solution.py:63
  151.5 5.8 %fusion.47 = (f32[768]{0:T(1024)S(1)}, f32[768]{0:T(1024)S(1)}, f32[768,1024]{1,0:T(8,128)}) fusion(bf16[1024,768]{1,0:T(8,128)(2,1)S(1)} %bitcast.56, bf16[1,1024,1024]{2,1,0:T(8,128)(2,1)} %all-gather.11.cloned.1.call-done, bf16[768,1024]{1,0:T(8,128)(2,1)} %param.7), kind=kOutput, calls=%fused_computation.70 | convolution fusion | flops 1615329792 | bytes 8394752 | tf_op jit(solution)/shard_map/dot_general | solution.py:61
  157.3 6.5 %all-reduce.1 = (f32[768]{0:T(1024)S(1)}, f32[768]{0:T(1024)S(1)}) all-reduce(f32[768]{0:T(1024)S(1)} %get-tuple-element.8, f32[768]{0:T(1024)S(1)} %get-tuple-element.7), channel_id=1, replica_groups=mesh['grp'=2,'sp'=4,'tp'=4] {'tp'}, use_global_device_ids=true, to_apply=%region_4.5 | all-reduce | flops 1536 | bytes 12288 | tf_op jit(solution)/shard_map/psum | solution.py:68
  163.8 33.6 %all-gather.13.cloned.1.call-done = bf16[1,1024,1024]{2,1,0:T(8,128)(2,1)} async-done(((bf16[1,256,1024]{2,1,0:T(8,128)(2,1)}), bf16[1,1024,1024]{2,1,0:T(8,128)(2,1)}) %all-gather.13.cloned.1.call-update) | async-done | bytes 2097168 | tf_op jit(solution)/shard_map/all_gather | solution.py:49
  197.4 5.6 %fusion.28 = bf16[1024,768]{1,0:T(8,128)(2,1)} fusion(bf16[1,1024,1024]{2,1,0:T(8,128)(2,1)} %all-gather.13.cloned.1.call-done, f32[768,1024]{1,0:T(8,128)} %get-tuple-element.27, f32[1024]{0:T(1024)S(1)} %bitcast.61, f32[1024]{0:T(1024)S(1)} %bitcast.59, f32[768]{0:T(1024)S(1)} %get-tuple-element.26, f32[768]{0:T(1024)S(1)} %get-tuple-element.25), kind=kOutput, calls=%fused_computation.42 | convolution fusion | flops 1615331328 | bytes 6830080 | tf_op jit(solution)/shard_map/dot_general | solution.py:50
  203.1 0.0 all-reduce.7.cloned.1.call-update
  203.1 0.0 all-gather.15.cloned.1.call-start
  203.1 0.5 all-gather.15.cloned.1.call-update
  203.7 41.2 %all-reduce.7.cloned.1.call-done = bf16[1024,768]{1,0:T(8,128)(2,1)} async-done(((bf16[1024,768]{1,0:T(8,128)(2,1)}), bf16[1024,768]{1,0:T(8,128)(2,1)}) %all-reduce.7.cloned.1.call-update) | async-done | bytes 1572880 | tf_op jit(solution)/shard_map/psum | solution.py:53
  244.9 1.1 slice.149
  246.0 3.6 %collective-permute-start.1 = (bf16[1024,15]{1,0:T(8,128)(2,1)S(1)}, bf16[1024,15]{1,0:T(8,128)(2,1)S(1)}, u32[]{:S(2)}, u32[]{:S(2)}) collective-permute-start(bf16[1024,15]{1,0:T(8,128)(2,1)S(1)} %slice.149), channel_id=1, source_target_pairs={{0,4},{4,8},{8,12},{1,5},{5,9},{9,13},{2,6},{6,10},{10,14},{3,7},{... | collective-permute-start | bytes 92168 | tf_op jit(solution)/shard_map/ppermute | solution.py:17
  249.6 5.5 %collective-permute-done.1 = bf16[1024,15]{1,0:T(8,128)(2,1)S(1)} collective-permute-done((bf16[1024,15]{1,0:T(8,128)(2,1)S(1)}, bf16[1024,15]{1,0:T(8,128)(2,1)S(1)}, u32[]{:S(2)}, u32[]{:S(2)}) %collective-permute-start.1) | collective-permute-done | bytes 30752 | tf_op jit(solution)/shard_map/ppermute | solution.py:17
  255.2 2.2 maximum_convert_fusion.1
  257.4 1.0 slice_add_fusion.2
  258.4 1.0 slice_add_fusion.1
  259.4 0.0 copy-start.1
  259.4 1.0 slice_add_fusion
  260.5 0.4 copy-done.1
  260.9 4.1 %fusion.3 = bf16[1024,768]{1,0:T(8,128)(2,1)S(1)} fusion(f32[1024,782]{1,0:T(8,128)S(1)} %slice_add_fusion.2, f32[1024,780]{1,0:T(8,128)S(1)} %slice_add_fusion.1, f32[1024,776]{1,0:T(8,128)S(1)} %slice_add_fusion, bf16[1024,768]{1,0:T(8,128)(2,1)S(1)} %copy-done.1, f32[1024]{0:T(1024)S(1)} %fusion.44, f32[768]{0:T(1024)S(1)} %add_convert_fusion.2, ...), kind=kLoop, calls=%fused_computation.11 | loop fusion | flops 7864320 | bytes 15739904 | tf_op jit(solution)/shard_map/convert_element_type | solution.py:38
  265.0 1.8 multiply_convert_fusion
  266.8 25.3 %all-gather.15.cloned.1.call-done = bf16[1,1024,1024]{2,1,0:T(8,128)(2,1)} async-done(((bf16[1,256,1024]{2,1,0:T(8,128)(2,1)}), bf16[1,1024,1024]{2,1,0:T(8,128)(2,1)}) %all-gather.15.cloned.1.call-update) | async-done | bytes 2097168 | tf_op jit(solution)/shard_map/all_gather | solution.py:63
  292.1 5.6 %fusion.46 = (f32[768]{0:T(1024)S(1)}, f32[768]{0:T(1024)S(1)}, f32[768,1024]{1,0:T(8,128)S(1)}) fusion(bf16[1024,768]{1,0:T(8,128)(2,1)} %bitcast.55, bf16[1,1024,1024]{2,1,0:T(8,128)(2,1)} %all-gather.15.cloned.1.call-done, f32[1024]{0:T(1024)S(1)} %bitcast.62, f32[1024]{0:T(1024)S(1)} %bitcast.60, f32[768]{0:T(1024)S(1)} %get-tuple-element.26, ...), kind=kOutput, calls=%fused_computation.69 | convolution fusion | flops 1619261952 | bytes 9981952 | tf_op jit(solution)/shard_map/dot_general | solution.py:61
  297.7 6.5 %all-reduce = (f32[768]{0:T(1024)S(1)}, f32[768]{0:T(1024)S(1)}) all-reduce(f32[768]{0:T(1024)S(1)} %get-tuple-element.6, f32[768]{0:T(1024)S(1)} %get-tuple-element.5), channel_id=1, replica_groups=mesh['grp'=2,'sp'=4,'tp'=4] {'tp'}, use_global_device_ids=true, to_apply=%region_9.10 | all-reduce | flops 1536 | bytes 12288 | tf_op jit(solution)/shard_map/psum | solution.py:68
  304.2 1.7 add_convert_fusion
  (11 shorter events, 0.1 us)
Async XLA Ops:
  6.5 50.8 %all-gather.9.cloned.1.call-start = ((), (), s32[]{:S(2)}) async-start(), calls=%async_computation.2 | async-start | bytes 2621440 | tf_op jit(solution)/shard_map/all_gather | solution.py:49
  8.8 53.6 %copy-start.2 = (bf16[2,256,1024]{2,1,0:T(8,128)(2,1)S(1)}, bf16[2,256,1024]{2,1,0:T(8,128)(2,1)}, u32[]{:S(2)}) copy-start(bf16[2,256,1024]{2,1,0:T(8,128)(2,1)} %param.9) | copy-start | bytes 3145732
  8.8 95.4 %all-reduce.5.cloned.1.call-start = ((), (), s32[]{:S(2)}) async-start(), calls=%async_computation | async-start | bytes 3145728 | tf_op jit(solution)/shard_map/psum | solution.py:53
  62.3 1.9 copy-start.4
  62.3 1.9 copy-start.5
  62.3 1.9 copy-start.6
  62.4 89.1 %all-gather.11.cloned.1.call-start = ((), (), s32[]{:S(2)}) async-start(), calls=%async_computation.3 | async-start | bytes 2621440 | tf_op jit(solution)/shard_map/all_gather | solution.py:63
  63.5 133.9 %all-gather.13.cloned.1.call-start = ((), (), s32[]{:S(2)}) async-start(), calls=%async_computation.4 | async-start | bytes 2621440 | tf_op jit(solution)/shard_map/all_gather | solution.py:49
  64.1 180.8 %all-reduce.7.cloned.1.call-start = ((), (), s32[]{:S(2)}) async-start(), calls=%async_computation.1 | async-start | bytes 3145728 | tf_op jit(solution)/shard_map/psum | solution.py:53
  105.3 8.8 %collective-permute-start = (bf16[1024,15]{1,0:T(8,128)(2,1)S(1)}, bf16[1024,15]{1,0:T(8,128)(2,1)S(1)}, u32[]{:S(2)}, u32[]{:S(2)}) collective-permute-start(bf16[1024,15]{1,0:T(8,128)(2,1)S(1)} %slice.138), channel_id=1, source_target_pairs={{0,4},{4,8},{8,12},{1,5},{5,9},{9,13},{2,6},{6,10},{10,14},{3,7},{... | collective-permute-start | bytes 92168 | tf_op jit(solution)/shard_map/ppermute | solution.py:17
  118.5 1.4 copy-start
  119.9 4.1 %copy-start.3 = (bf16[2,4,256,256]{3,2,1,0:T(8,128)(2,1)S(1)}, bf16[2,4,256,256]{3,2,1,0:T(8,128)(2,1)}, u32[]{:S(2)}) copy-start(bf16[2,4,256,256]{3,2,1,0:T(8,128)(2,1)} %param.10) | copy-start | bytes 3145732
  203.1 89.0 %all-gather.15.cloned.1.call-start = ((), (), s32[]{:S(2)}) async-start(), calls=%async_computation.5 | async-start | bytes 2621440 | tf_op jit(solution)/shard_map/all_gather | solution.py:63
  246.0 9.2 %collective-permute-start.1 = (bf16[1024,15]{1,0:T(8,128)(2,1)S(1)}, bf16[1024,15]{1,0:T(8,128)(2,1)S(1)}, u32[]{:S(2)}, u32[]{:S(2)}) collective-permute-start(bf16[1024,15]{1,0:T(8,128)(2,1)S(1)} %slice.149), channel_id=1, source_target_pairs={{0,4},{4,8},{8,12},{1,5},{5,9},{9,13},{2,6},{6,10},{10,14},{3,7},{... | collective-permute-start | bytes 92168 | tf_op jit(solution)/shard_map/ppermute | solution.py:17
  259.4 1.4 copy-start.1
Sparse Core Ops, SparseCore 0:
  8.9 48.3 all-gather.8
  62.5 41.6 all-reduce.4
  105.8 45.7 all-gather.10
  152.9 44.4 all-gather.12
  203.2 41.6 all-reduce.6
  246.3 45.7 all-gather.14
where the time goes:
time: 313 us
  waiting for transfers between devices  227 us (73%)
  matrix products  24.5 us (8%)
  other arithmetic  20.6 us (7%)
  between operations  13.7 us (4%)
  blocking collectives  13 us (4%)
  starting transfers between devices  7.2 us (2%)
  local copies, waits for them, and re-layouts  6.35 us (2%)
    all_gather x2, waiting for transfers between devices, per_device(): whole_in = lax.all_gather(in_weight[layer_index], 'sp', axis=0, tiled=True)  82.1 us
    psum x2, waiting for transfers between devices, per_device(): hidden = lax.psum(partial_value.astype(jnp.bfloat16), 'tp')  81.1 us
    all_gather x2, waiting for transfers between devices, per_device(): lax.all_gather(out_weight[layer_index], 'sp', axis=0, tiled=True)  52.2 us
    psum x2, blocking collectives, per_device(): lax.psum((jnp.sum(summed, axis=1), jnp.sum(summed * summed, axis=1)), 'tp')  13 us
    dot_general x2, matrix products, per_device(): lax.dot_general(scaled, lax.all_gather(out_weight[layer_index], 'sp', axi...  11.4 us
    ppermute x2, waiting for transfers between devices, passed_along(): return lax.ppermute(block, axis, route)  10.9 us
    dot_general x2, matrix products, per_device(): lax.dot_general(whole_in, current, contract_cols, preferred_element_type=...  10.6 us
    convert_element_type x2, other arithmetic, pooled_windows(): (window_sums / counts - hidden.astype(jnp.float32)).astype(jnp.bfloat16)  8.26 us
  transfers between devices with their start and end apart: 8, of which 8 were waited for; matrix products, arithmetic and copies ran while one was open for 10% of the time, Pallas kernels for 0%

commit v1 on v0

--- a/solution.py
+++ b/solution.py
@@ -1,7 +1,9 @@
+import functools
 import jax
 import jax.numpy as jnp
 from jax import lax
 from jax.sharding import PartitionSpec as P
+from jax.lax import all_to_all, psum
 
 D = 4096
 POOL = 1024
@@ -9,6 +11,19 @@
 GROUP_WIDTH = 256
 LAYERS = 2
 epsilon = 1e-05
+
+
+def finish_the_inputs(slab_in, which_axis):
+    table = []
+    for _ in range(psum(1, which_axis)):
+        table.append(slab_in)
+    v_now = jnp.stack(table)
+    g_now = all_to_all(v_now, which_axis, 0, 0)
+    u_next = jnp.concatenate(g_now, axis=0)
+    return u_next
+
+
+divide_task_up = functools.partial(finish_the_inputs, which_axis="sp")
 
 
 def passed_along(block, axis, distance):
@@ -46,7 +61,7 @@
     contract_cols = (((1,), (1,)), ((), ()))
     current = stream
     for layer_index in range(LAYERS):
-        whole_in = lax.all_gather(in_weight[layer_index], "sp", axis=0, tiled=True)
+        whole_in = divide_task_up(in_weight[layer_index])
         partial_value = lax.dot_general(
             whole_in, current, contract_cols, preferred_element_type=jnp.float32
         )

time: 313 us -> 272 us (0.87)
  waiting for transfers between devices: 227 us -> 128 us
  blocking collectives: 13 us -> 66.5 us
  starting transfers between devices: 7.2 us -> 10.7 us
    all_gather x2 -> x0, waiting for transfers between devices: 82.1 us -> none  [per_device(): whole_in = lax.all_gather(in_weight[layer_index], 'sp', axis=0, tiled=True)]
    all_to_all x0 -> x1, blocking collectives: none -> 54.5 us  [finish_the_inputs(): g_now = all_to_all(v_now, which_axis, 0, 0)]
    all_gather x2, waiting for transfers between devices: 52.2 us -> 0.01 us  [per_device(): lax.all_gather(out_weight[layer_index], 'sp', axis=0, tiled=True)]
    ppermute x2, waiting for transfers between devices: 10.9 us -> 31.6 us  [passed_along(): return lax.ppermute(block, axis, route)]
    psum x2, waiting for transfers between devices: 81.1 us -> 95.4 us  [per_device(): hidden = lax.psum(partial_value.astype(jnp.bfloat16), 'tp')]
    all_to_all x0 -> x1, starting transfers between devices: none -> 3.76 us  [finish_the_inputs(): g_now = all_to_all(v_now, which_axis, 0, 0)]
  transfers between devices with their start and end apart: 8 -> 7, of which waited for: 8 -> 4; matrix products, arithmetic and copies ran while one was open for 10% -> 12% of each run, Pallas kernels for 0% -> 0%
where the time goes in v1:
time: 272 us; the launch traced here: 271 us
  waiting for transfers between devices  128 us (47%)
  blocking collectives  66.5 us (24%)
  matrix products  23.4 us (9%)
  other arithmetic  20.6 us (8%)
  between operations  15.1 us (6%)
  starting transfers between devices  10.7 us (4%)
  local copies, waits for them, and re-layouts  7.23 us (3%)
    psum x2, waiting for transfers between devices, per_device(): hidden = lax.psum(partial_value.astype(jnp.bfloat16), 'tp')  95.4 us
    all_to_all x1, blocking collectives, finish_the_inputs(): g_now = all_to_all(v_now, which_axis, 0, 0)  54.5 us
    ppermute x2, waiting for transfers between devices, passed_along(): return lax.ppermute(block, axis, route)  31.6 us
    psum x2, blocking collectives, per_device(): lax.psum((jnp.sum(summed, axis=1), jnp.sum(summed * summed, axis=1)), 'tp')  12 us
    dot_general x2, matrix products, per_device(): lax.dot_general(scaled, lax.all_gather(out_weight[layer_index], 'sp', axi...  11.9 us
    convert_element_type x2, other arithmetic, pooled_windows(): (window_sums / counts - hidden.astype(jnp.float32)).astype(jnp.bfloat16)  8.29 us
    dot_general x2, matrix products, per_device(): lax.dot_general(whole_in, current, contract_cols, preferred_element_type=...  7.97 us
    ppermute x2, starting transfers between devices, passed_along(): return lax.ppermute(block, axis, route)  6.81 us
  transfers between devices with their start and end apart: 7, of which 4 were waited for; matrix products, arithmetic and copies ran while one was open for 12% of the time, Pallas kernels for 0%

profile of v1, /device:TPU:0, one launch (start us, length us, event | category | flops | bytes accessed | tf_op | source)
XLA Modules:
  0.0 271.2 jit_solution(13875615155138149304)
XLA Ops:
  7.4 0.0 all-reduce.5.cloned.1.call-start
  7.4 1.3 slice_bitcast_fusion.1
  8.6 0.0 copy-start.7
  8.7 0.3 stack.6
  8.9 54.5 %all_to_all.10 = bf16[4,256,1024]{2,1,0:T(8,128)(2,1)S(1)} all-to-all(bf16[4,256,1024]{2,1,0:T(8,128)(2,1)S(1)} %stack.6), channel_id=1, replica_groups=mesh['grp'=2,'sp'=4,'tp'=4] {'sp'}, dimensions={0} | all-to-all | bytes 4194304 | tf_op jit(solution)/shard_map/all_to_all | solution.py:21
  63.4 0.0 copy-done.7
  63.4 3.0 %convolution_convert_fusion.1 = bf16[1024,768]{1,0:T(8,128)(2,1)} fusion(bf16[1024,1024]{1,0:T(8,128)(2,1)S(1)} %bitcast.52, bf16[768,1024]{1,0:T(8,128)(2,1)S(1)} %copy-done.7), kind=kOutput, calls=%fused_computation.37 | convolution fusion | flops 1611399168 | bytes 5242880 | tf_op jit(solution)/shard_map/dot_general | solution.py:65
  66.4 0.0 all-reduce.5.cloned.1.call-update
  66.4 0.0 copy-start.2
  66.4 1.6 stack.7
  68.0 0.0 copy-start.4
  68.0 0.0 copy-start.5
  68.0 0.0 copy-start.6
  68.0 3.8 %all-to-all-start.1 = ((bf16[4,256,1024]{2,1,0:T(8,128)(2,1)}), bf16[4,256,1024]{2,1,0:T(8,128)(2,1)S(1)}, u32[]{:S(2)}, u32[]{:S(2)}) async-start(bf16[4,256,1024]{2,1,0:T(8,128)(2,1)} %stack.7), calls=%async_computation.1 | async-start | bytes 4194304 | tf_op jit(solution)/shard_map/all_to_all | solution.py:21
  71.8 0.0 all-gather.5.cloned.1.call-start
  71.9 0.0 copy-done.2
  71.9 1.1 fusion.36
  72.9 0.0 all-gather.5.cloned.1.call-update
  73.0 0.0 all-reduce.7.cloned.1.call-start
  73.0 0.0 copy-done.4
  73.1 0.0 copy-done.5
  73.1 0.0 copy-done.6
  73.1 35.5 %all-reduce.5.cloned.1.call-done = bf16[1024,768]{1,0:T(8,128)(2,1)} async-done(((bf16[1024,768]{1,0:T(8,128)(2,1)}), bf16[1024,768]{1,0:T(8,128)(2,1)}) %all-reduce.5.cloned.1.call-update) | async-done | bytes 1572880 | tf_op jit(solution)/shard_map/psum | solution.py:68
  108.6 1.1 slice.144
  109.7 3.4 %collective-permute-start = (bf16[1024,15]{1,0:T(8,128)(2,1)S(1)}, bf16[1024,15]{1,0:T(8,128)(2,1)S(1)}, u32[]{:S(2)}, u32[]{:S(2)}) collective-permute-start(bf16[1024,15]{1,0:T(8,128)(2,1)S(1)} %slice.144), channel_id=1, source_target_pairs={{0,4},{4,8},{8,12},{1,5},{5,9},{9,13},{2,6},{6,10},{10,14},{3,7},{... | collective-permute-start | bytes 92168 | tf_op jit(solution)/shard_map/ppermute | solution.py:32
  113.2 26.2 %collective-permute-done = bf16[1024,15]{1,0:T(8,128)(2,1)S(1)} collective-permute-done((bf16[1024,15]{1,0:T(8,128)(2,1)S(1)}, bf16[1024,15]{1,0:T(8,128)(2,1)S(1)}, u32[]{:S(2)}, u32[]{:S(2)}) %collective-permute-start) | collective-permute-done | bytes 30752 | tf_op jit(solution)/shard_map/ppermute | solution.py:32
  139.4 2.2 maximum_convert_fusion
  141.7 1.0 slice_add_fusion.5
  142.7 1.0 slice_add_fusion.4
  143.7 0.0 copy-start
  143.7 1.0 slice_add_fusion.3
  144.7 0.4 copy-done
  145.1 0.0 copy-start.3
  145.1 4.1 %fusion.1 = bf16[1024,768]{1,0:T(8,128)(2,1)S(1)} fusion(f32[1024,782]{1,0:T(8,128)S(1)} %slice_add_fusion.5, f32[1024,780]{1,0:T(8,128)S(1)} %slice_add_fusion.4, f32[1024,776]{1,0:T(8,128)S(1)} %slice_add_fusion.3, bf16[1024,768]{1,0:T(8,128)(2,1)S(1)} %copy-done, f32[1024]{0:T(1024)S(1)} %fusion.32, f32[768]{0:T(1024)S(1)} %add_convert_fusion.2, ...), kind=kLoop, calls=%fused_computation.9 | loop fusion | flops 7864320 | bytes 15739904 | tf_op jit(solution)/shard_map/convert_element_type | solution.py:53
  149.2 0.0 copy-done.3
  149.3 1.8 multiply_convert_fusion.1
  151.0 0.0 all-gather.5.cloned.1.call-done
  151.1 6.3 %fusion.35 = (f32[768]{0:T(1024)S(1)}, f32[768]{0:T(1024)S(1)}, f32[768,1024]{1,0:T(8,128)}) fusion(bf16[1024,768]{1,0:T(8,128)(2,1)} %bitcast.54, bf16[1,1024,1024]{2,1,0:T(8,128)(2,1)} %all-gather.5.cloned.1.call-done, bf16[768,1024]{1,0:T(8,128)(2,1)} %param.7), kind=kOutput, calls=%fused_computation.68 | convolution fusion | flops 1615329792 | bytes 8394752 | tf_op jit(solution)/shard_map/dot_general | solution.py:76
  157.3 5.9 %all-reduce.1 = (f32[768]{0:T(1024)S(1)}, f32[768]{0:T(1024)S(1)}) all-reduce(f32[768]{0:T(1024)S(1)} %get-tuple-element.8, f32[768]{0:T(1024)S(1)} %get-tuple-element.7), channel_id=1, replica_groups=mesh['grp'=2,'sp'=4,'tp'=4] {'tp'}, use_global_device_ids=true, to_apply=%region_4.5 | all-reduce | flops 1536 | bytes 12288 | tf_op jit(solution)/shard_map/psum | solution.py:83
  163.3 0.0 all-to-all-done.1
  163.3 5.0 %fusion.18 = bf16[1024,768]{1,0:T(8,128)(2,1)} fusion(bf16[1024,1024]{1,0:T(8,128)(2,1)S(1)} %bitcast.51, f32[768,1024]{1,0:T(8,128)} %get-tuple-element.27, f32[1024]{0:T(1024)S(1)} %bitcast.59, f32[1024]{0:T(1024)S(1)} %bitcast.57, f32[768]{0:T(1024)S(1)} %get-tuple-element.26, f32[768]{0:T(1024)S(1)} %get-tuple-element.25), kind=kOutput, calls=%fused_computation.38 | convolution fusion | flops 1615331328 | bytes 6830080 | tf_op jit(solution)/shard_map/dot_general | solution.py:65
  168.3 0.0 all-reduce.7.cloned.1.call-update
  168.3 0.0 all-gather.7.cloned.1.call-start
  168.3 0.5 all-gather.7.cloned.1.call-update
  168.9 59.9 %all-reduce.7.cloned.1.call-done = bf16[1024,768]{1,0:T(8,128)(2,1)} async-done(((bf16[1024,768]{1,0:T(8,128)(2,1)}), bf16[1024,768]{1,0:T(8,128)(2,1)}) %all-reduce.7.cloned.1.call-update) | async-done | bytes 1572880 | tf_op jit(solution)/shard_map/psum | solution.py:68
  228.8 1.1 slice.155
  229.9 3.4 %collective-permute-start.1 = (bf16[1024,15]{1,0:T(8,128)(2,1)S(1)}, bf16[1024,15]{1,0:T(8,128)(2,1)S(1)}, u32[]{:S(2)}, u32[]{:S(2)}) collective-permute-start(bf16[1024,15]{1,0:T(8,128)(2,1)S(1)} %slice.155), channel_id=1, source_target_pairs={{0,4},{4,8},{8,12},{1,5},{5,9},{9,13},{2,6},{6,10},{10,14},{3,7},{... | collective-permute-start | bytes 92168 | tf_op jit(solution)/shard_map/ppermute | solution.py:32
  233.3 5.4 %collective-permute-done.1 = bf16[1024,15]{1,0:T(8,128)(2,1)S(1)} collective-permute-done((bf16[1024,15]{1,0:T(8,128)(2,1)S(1)}, bf16[1024,15]{1,0:T(8,128)(2,1)S(1)}, u32[]{:S(2)}, u32[]{:S(2)}) %collective-permute-start.1) | collective-permute-done | bytes 30752 | tf_op jit(solution)/shard_map/ppermute | solution.py:32
  238.7 2.2 maximum_convert_fusion.1
  241.0 1.0 slice_add_fusion.2
  242.0 1.0 slice_add_fusion.1
  243.0 0.0 copy-start.1
  243.0 1.0 slice_add_fusion
  244.0 0.4 copy-done.1
  244.4 4.1 %fusion.3 = bf16[1024,768]{1,0:T(8,128)(2,1)S(1)} fusion(f32[1024,782]{1,0:T(8,128)S(1)} %slice_add_fusion.2, f32[1024,780]{1,0:T(8,128)S(1)} %slice_add_fusion.1, f32[1024,776]{1,0:T(8,128)S(1)} %slice_add_fusion, bf16[1024,768]{1,0:T(8,128)(2,1)S(1)} %copy-done.1, f32[1024]{0:T(1024)S(1)} %fusion.32, f32[768]{0:T(1024)S(1)} %add_convert_fusion.2, ...), kind=kLoop, calls=%fused_computation.11 | loop fusion | flops 7864320 | bytes 15739904 | tf_op jit(solution)/shard_map/convert_element_type | solution.py:53
  248.6 1.8 multiply_convert_fusion
  250.4 0.0 all-gather.7.cloned.1.call-done
  250.4 5.6 %fusion.34 = (f32[768]{0:T(1024)S(1)}, f32[768]{0:T(1024)S(1)}, f32[768,1024]{1,0:T(8,128)S(1)}) fusion(bf16[1024,768]{1,0:T(8,128)(2,1)} %bitcast.53, bf16[1,1024,1024]{2,1,0:T(8,128)(2,1)} %all-gather.7.cloned.1.call-done, f32[1024]{0:T(1024)S(1)} %bitcast.60, f32[1024]{0:T(1024)S(1)} %bitcast.58, f32[768]{0:T(1024)S(1)} %get-tuple-element.26, ...), kind=kOutput, calls=%fused_computation.67 | convolution fusion | flops 1619261952 | bytes 9981952 | tf_op jit(solution)/shard_map/dot_general | solution.py:76
  256.0 6.1 %all-reduce = (f32[768]{0:T(1024)S(1)}, f32[768]{0:T(1024)S(1)}) all-reduce(f32[768]{0:T(1024)S(1)} %get-tuple-element.6, f32[768]{0:T(1024)S(1)} %get-tuple-element.5), channel_id=1, replica_groups=mesh['grp'=2,'sp'=4,'tp'=4] {'tp'}, use_global_device_ids=true, to_apply=%region_9.10 | all-reduce | flops 1536 | bytes 12288 | tf_op jit(solution)/shard_map/psum | solution.py:83
  262.1 1.7 add_convert_fusion
  (11 shorter events, 0.1 us)
Async XLA Ops:
  7.4 101.3 %all-reduce.5.cloned.1.call-start = ((), (), s32[]{:S(2)}) async-start(), calls=%async_computation.2 | async-start | bytes 3145728 | tf_op jit(solution)/shard_map/psum | solution.py:68
  8.6 54.8 %copy-start.7 = (bf16[768,1024]{1,0:T(8,128)(2,1)S(1)}, bf16[768,1024]{1,0:T(8,128)(2,1)}, u32[]{:S(2)}) copy-start(bf16[768,1024]{1,0:T(8,128)(2,1)} %param.7) | copy-start | bytes 4718596
  66.4 5.5 %copy-start.2 = (bf16[2,256,1024]{2,1,0:T(8,128)(2,1)S(1)}, bf16[2,256,1024]{2,1,0:T(8,128)(2,1)}, u32[]{:S(2)}) copy-start(bf16[2,256,1024]{2,1,0:T(8,128)(2,1)} %param.9) | copy-start | bytes 3145732
  68.0 5.0 %copy-start.4 = (f32[2,1024]{1,0:T(2,128)S(1)}, f32[2,1024]{1,0:T(2,128)}, u32[]{:S(2)}) copy-start(f32[2,1024]{1,0:T(2,128)} %param.11) | copy-start | bytes 24580
  68.0 5.0 %copy-start.5 = (f32[2,1024]{1,0:T(2,128)S(1)}, f32[2,1024]{1,0:T(2,128)}, u32[]{:S(2)}) copy-start(f32[2,1024]{1,0:T(2,128)} %param.12) | copy-start | bytes 24580
  68.0 5.1 %copy-start.6 = (f32[2,1024]{1,0:T(2,128)S(1)}, f32[2,1024]{1,0:T(2,128)}, u32[]{:S(2)}) copy-start(f32[2,1024]{1,0:T(2,128)} %param.13) | copy-start | bytes 24580
  68.0 95.2 %all-to-all-start.1 = ((bf16[4,256,1024]{2,1,0:T(8,128)(2,1)}), bf16[4,256,1024]{2,1,0:T(8,128)(2,1)S(1)}, u32[]{:S(2)}, u32[]{:S(2)}) async-start(bf16[4,256,1024]{2,1,0:T(8,128)(2,1)} %stack.7), calls=%async_computation.1 | async-start | bytes 4194304 | tf_op jit(solution)/shard_map/all_to_all | solution.py:21
  71.8 79.2 %all-gather.5.cloned.1.call-start = ((), (), s32[]{:S(2)}) async-start(), calls=%async_computation.4 | async-start | bytes 2621440 | tf_op jit(solution)/shard_map/all_gather | solution.py:78
  73.0 155.9 %all-reduce.7.cloned.1.call-start = ((), (), s32[]{:S(2)}) async-start(), calls=%async_computation.3 | async-start | bytes 3145728 | tf_op jit(solution)/shard_map/psum | solution.py:68
  109.7 29.7 %collective-permute-start = (bf16[1024,15]{1,0:T(8,128)(2,1)S(1)}, bf16[1024,15]{1,0:T(8,128)(2,1)S(1)}, u32[]{:S(2)}, u32[]{:S(2)}) collective-permute-start(bf16[1024,15]{1,0:T(8,128)(2,1)S(1)} %slice.144), channel_id=1, source_target_pairs={{0,4},{4,8},{8,12},{1,5},{5,9},{9,13},{2,6},{6,10},{10,14},{3,7},{... | collective-permute-start | bytes 92168 | tf_op jit(solution)/shard_map/ppermute | solution.py:32
  143.7 1.4 copy-start
  145.1 4.2 %copy-start.3 = (bf16[2,4,256,256]{3,2,1,0:T(8,128)(2,1)S(1)}, bf16[2,4,256,256]{3,2,1,0:T(8,128)(2,1)}, u32[]{:S(2)}) copy-start(bf16[2,4,256,256]{3,2,1,0:T(8,128)(2,1)} %param.10) | copy-start | bytes 3145732
  168.3 82.1 %all-gather.7.cloned.1.call-start = ((), (), s32[]{:S(2)}) async-start(), calls=%async_computation.5 | async-start | bytes 2621440 | tf_op jit(solution)/shard_map/all_gather | solution.py:78
  229.9 8.8 %collective-permute-start.1 = (bf16[1024,15]{1,0:T(8,128)(2,1)S(1)}, bf16[1024,15]{1,0:T(8,128)(2,1)S(1)}, u32[]{:S(2)}, u32[]{:S(2)}) collective-permute-start(bf16[1024,15]{1,0:T(8,128)(2,1)S(1)} %slice.155), channel_id=1, source_target_pairs={{0,4},{4,8},{8,12},{1,5},{5,9},{9,13},{2,6},{6,10},{10,14},{3,7},{... | collective-permute-start | bytes 92168 | tf_op jit(solution)/shard_map/ppermute | solution.py:32
  243.0 1.4 copy-start.1
Sparse Core Ops, SparseCore 0:
  66.5 42.0 all-reduce.4
  168.4 60.3 all-reduce.6
Sparse Core Ops, SparseCore 1:
  73.9 75.9 all-gather.4
  170.3 63.0 all-gather.6
